TPU v7x, 32 devices: a whole 2x2x4 slice. The times are simulated.
32 devices in a mesh: kv: 8 (over z, y), tp: 4 (over x, core).
Axes of the slice: x: 2, y: 2, z: 4, core: 2. Of those that a mesh axis runs over, the one named last changes fastest.
Arguments:
- tokens: bfloat16 [8, 2048], P(None, 'kv'), may hold values from -6 to 6
- in_gain: float32 [2048], P('kv'), may hold values from 0.1 to 1.9
- w_query: bfloat16 [2048, 512], P('kv', 'tp'), may hold values from -0.125 to 0.125
- score_bias: float32 [4], P('tp'), as said below
- cache_keys: bfloat16 [8, 8192, 512], P(None, 'kv', 'tp'), may hold values from -8 to 8, as said below
- cache_values: bfloat16 [8, 8192, 512], P(None, 'kv', 'tp'), may hold values from -6 to 6
- lengths: int32 [8], replicated, may hold values from 1024 to 8192, as said below
- head_gain: float32 [512], P('tp'), may hold values from 0.1 to 1.9
- w_out: bfloat16 [512, 2048], P('tp', 'kv'), may hold values from -0.25 to 0.25
Outputs:
- mixed: bfloat16 [8, 2048], P(None, 'kv')
Inputs may be any that keep to these rules, and one draw needn't show every extreme that they name: `score_bias`: one value a head, added to every score of that head. `cache_keys`: real-valued key entries. `lengths`: one sequence has all 8192 positions cached.
All inputs are finite; a program needn't handle non-finite values.
Results may differ from a plain program's by a relative error of at most 0.0095.
The roundings to bfloat16 on the way count: a program that leaves them out, or rounds other values in their place, can miss the bound.
Values may be sent and summed in bfloat16 or wider, within the bound.
No kernel may reach another device: no remote copies, remote signals or barrier semaphores. Data moves between devices by JAX's collectives and lax.ppermute only.
A program may use at most 64 MiB of HBM per device.

v0:
```python
import jax
import jax.numpy as jnp
from jax import lax
from jax.sharding import PartitionSpec as P

D = 2048
EPS = 1e-06


def shards(
    tokens, in_gain, w_query, score_bias, cache_keys, cache_values, lengths, head_gain, w_out
):
    sequences = tokens.shape[0]
    local_len = cache_keys.shape[1]
    head_width = cache_keys.shape[2]
    heads_here = score_bias.shape[0]
    head_size = head_width // heads_here
    as_float = tokens.astype(jnp.float32)
    gained = (as_float * in_gain).astype(jnp.bfloat16)
    partial_value = jnp.dot(gained, w_query, preferred_element_type=jnp.float32)
    squares = jnp.sum(as_float * as_float, axis=1)
    summed, total_sq = lax.psum((partial_value, squares), "kv")
    row_scale = lax.rsqrt(total_sq / D + EPS)
    queries = (
        (summed * row_scale[:, None]).astype(jnp.bfloat16).reshape(sequences, heads_here, head_size)
    )
    key_heads = cache_keys.reshape(sequences, local_len, heads_here, head_size)
    value_heads = cache_values.reshape(sequences, local_len, heads_here, head_size)
    scores = jnp.einsum("bhd,bphd->bhp", queries, key_heads, preferred_element_type=jnp.float32)
    scores = scores * head_size ** (-0.5) + score_bias[None, :, None]
    offset = lax.axis_index("kv") * local_len
    places = offset + lax.iota(jnp.int32, local_len)
    usable = places[None, None, :] < lengths[:, None, None]
    log_keep = jnp.where(usable, jax.nn.log_sigmoid(-scores), 0.0)
    strict_upper = (
        lax.iota(jnp.int32, local_len)[:, None] > lax.iota(jnp.int32, local_len)[None, :]
    ).astype(jnp.float32)
    suffix = jnp.einsum("bhr,rs->bhs", log_keep, strict_upper, precision=lax.Precision.HIGHEST)
    weights = jnp.where(usable, jnp.exp(jax.nn.log_sigmoid(scores) + suffix), 0.0).astype(
        jnp.bfloat16
    )
    local_out = jnp.einsum(
        "bhp,bphd->bhd", weights, value_heads, preferred_element_type=jnp.float32
    )
    seg_total = jnp.sum(log_keep, axis=2)
    every_total = lax.all_gather(seg_total[None], "kv", axis=0, tiled=True)
    ranks_kv = lax.iota(jnp.int32, every_total.shape[0])
    later_sum = jnp.sum(
        jnp.where((ranks_kv > lax.axis_index("kv"))[:, None, None], every_total, 0.0), axis=0
    )
    attended = lax.psum(local_out * jnp.exp(later_sum)[..., None], "kv")
    mean_sq = jnp.mean(attended * attended, axis=2)
    normed = attended * lax.rsqrt(mean_sq + EPS)[..., None]
    normed = (normed.reshape(sequences, head_width) * head_gain).astype(jnp.bfloat16)
    part_out = jnp.dot(normed, w_out, preferred_element_type=jnp.float32)
    return lax.psum(part_out.astype(jnp.bfloat16), "tp")


def solution(mesh):
    return jax.shard_map(
        shards,
        mesh=mesh,
        in_specs=(
            P(None, "kv"),
            P("kv"),
            P("kv", "tp"),
            P("tp"),
            P(None, "kv", "tp"),
            P(None, "kv", "tp"),
            P(),
            P("tp"),
            P("tp", "kv"),
        ),
        out_specs=P(None, "kv"),
        check_vma=False,
    )
```

profile of v0, /device:TPU:0, one launch (start us, length us, event | category | flops | bytes accessed | tf_op | source)
XLA Modules:
  0.0 74.4 jit_solution(1985934041813011728)
XLA Ops:
  0.0 0.0 copy-start
  0.0 0.0 copy-start.4
  0.0 0.0 copy-start.1
  0.0 1.2 %fusion.19 = f32[8,128]{1,0:T(8,128)S(1)} fusion(bf16[256,128]{1,0:T(8,128)(2,1)} %param.11, bf16[8,256]{1,0:T(8,128)(2,1)} %param.9, f32[256]{0:T(256)} %param.10), kind=kOutput, calls=%fused_computation.27 | convolution fusion | flops 530432 | bytes 74752 | tf_op jit(solution)/shard_map/dot_general | solution.py:20
  1.2 0.8 %fusion.18 = f32[8]{0:T(128)S(1)} fusion(bf16[8,256]{1,0:T(8,128)(2,1)} %param.9), kind=kLoop, calls=%fused_computation.26 | loop fusion | flops 6136 | bytes 4128 | tf_op jit(solution)/shard_map/reduce_sum | solution.py:21
  2.0 23.4 %all-reduce.1 = (f32[8,128]{1,0:T(8,128)S(1)}, f32[8]{0:T(128)S(1)}) all-reduce(f32[8,128]{1,0:T(8,128)S(1)} %fusion.19, f32[8]{0:T(128)S(1)} %fusion.18), channel_id=1, replica_groups=mesh['kv'=8,'tp'=4] {'kv'}, use_global_device_ids=true, to_apply=%region_0.0 | all-reduce | flops 1032 | bytes 8256 | tf_op jit(solution)/shard_map/psum | solution.py:22
  25.4 0.1 fusion.25
  25.5 0.0 copy-done
  25.5 0.6 fusion.22
  26.1 0.0 copy-start.2
  26.1 0.0 copy-start.3
  26.8 0.0 copy-done.1
  26.8 0.2 fusion.11
  27.0 0.0 copy-done.4
  27.0 0.7 dynamic-slice
  28.4 0.2 dynamic-update-slice
  28.6 17.1 %all-reduce = f32[64]{0:T(128)S(1)} all-reduce(f32[64]{0:T(128)S(1)} %dynamic-update-slice), channel_id=2, replica_groups=mesh['kv'=8,'tp'=4] {'kv'}, use_global_device_ids=true, to_apply=%add | all-reduce | flops 64 | bytes 512
  45.7 0.1 reshape.93
  45.8 0.1 select_reduce_fusion
  45.9 0.7 fusion.5
  46.7 2.0 %fusion.9 = f32[8,1,128]{2,1,0:T(1,128)S(1)} fusion(bf16[8,1024,128]{2,1,0:T(8,128)(2,1)} %param.14, bf16[8,1024,1]{1,0,2:T(8,128)(2,1)S(1)} %fusion.5), kind=kOutput, calls=%fused_computation.15 | convolution fusion | flops 2097152 | bytes 2117632 | tf_op jit(solution)/shard_map/bhp,bphd->bhd/dot_general | solution.py:42
  48.6 0.1 multiply_bitcast_fusion
  48.7 19.1 %psum.30 = f32[8,1,128]{2,0,1:T(8,128)S(1)} all-reduce(f32[8,1,128]{2,0,1:T(8,128)S(1)} %multiply_bitcast_fusion), channel_id=1, replica_groups=mesh['kv'=8,'tp'=4] {'kv'}, use_global_device_ids=true, to_apply=%region_5.6 | all-reduce | flops 1024 | bytes 8192 | tf_op jit(solution)/shard_map/psum | solution.py:51
  67.8 0.1 multiply_reduce_fusion
  68.0 0.0 copy-done.2
  68.0 0.0 copy-done.3
  68.0 0.2 convolution_convert_fusion
  68.2 6.2 %psum.31 = bf16[8,256]{1,0:T(8,128)(2,1)} all-reduce(bf16[8,256]{1,0:T(8,128)(2,1)S(1)} %convolution_convert_fusion), channel_id=1, replica_groups=mesh['kv'=8,'tp'=4] {'tp'}, use_global_device_ids=true, to_apply=%region_7.8 | all-reduce | flops 2048 | bytes 8192 | tf_op jit(solution)/shard_map/psum | solution.py:56
  (6 shorter events, 0.0 us)
Async XLA Ops:
  0.0 25.5 %copy-start = (bf16[8,1024,128]{2,1,0:T(8,128)(2,1)S(1)}, bf16[8,1024,128]{2,1,0:T(8,128)(2,1)}, u32[]{:S(2)}) copy-start(bf16[8,1024,128]{2,1,0:T(8,128)(2,1)} %param.13) | copy-start | bytes 6291460
  0.0 27.0 %copy-start.4 = (u32[32]{0:T(128)S(1)}, u32[32]{0:T(128)}, u32[]{:S(2)}) copy-start(u32[32]{0:T(128)} %constant.28) | copy-start | bytes 388
  0.0 26.8 %copy-start.1 = (s32[8]{0:T(128)S(1)}, s32[8]{0:T(128)}, u32[]{:S(2)}) copy-start(s32[8]{0:T(128)} %param.15) | copy-start | bytes 100
  26.1 41.9 %copy-start.2 = (bf16[128,256]{1,0:T(8,128)(2,1)S(1)}, bf16[128,256]{1,0:T(8,128)(2,1)}, u32[]{:S(2)}) copy-start(bf16[128,256]{1,0:T(8,128)(2,1)} %param.17) | copy-start | bytes 196612
  26.1 41.9 %copy-start.3 = (f32[128]{0:T(128)S(1)}, f32[128]{0:T(128)}, u32[]{:S(2)}) copy-start(f32[128]{0:T(128)} %param.16) | copy-start | bytes 1540
where the time goes:
time: 74.7 us; the launch traced here: 74.4 us
  blocking collectives  65.9 us (88%)
  matrix products  4.69 us (6%)
  between operations  1.47 us (2%)
  other arithmetic  1.37 us (2%)
  local copies, waits for them, and re-layouts  1.01 us (1%)
    psum x1, blocking collectives, shards(): summed, total_sq = lax.psum((partial_value, squares), 'kv')  23.4 us
    psum x1, blocking collectives, shards(): attended = lax.psum(local_out * jnp.exp(later_sum)[..., None], 'kv')  19.1 us
    unnamed x1, blocking collectives  17.1 us
    psum x1, blocking collectives, shards(): return lax.psum(part_out.astype(jnp.bfloat16), 'tp')  6.23 us
    dot_general x1, matrix products, shards(): jnp.einsum('bhp,bphd->bhd', weights, value_heads, preferred_element_type=...  1.98 us

commit v1 on v0

--- a/solution.py
+++ b/solution.py
@@ -48,7 +48,7 @@
     later_sum = jnp.sum(
         jnp.where((ranks_kv > lax.axis_index("kv"))[:, None, None], every_total, 0.0), axis=0
     )
-    attended = lax.psum(local_out * jnp.exp(later_sum)[..., None], "kv")
+    attended = jnp.sum(lax.all_gather(local_out * jnp.exp(later_sum)[..., None], "kv"), axis=0)
     mean_sq = jnp.mean(attended * attended, axis=2)
     normed = attended * lax.rsqrt(mean_sq + EPS)[..., None]
     normed = (normed.reshape(sequences, head_width) * head_gain).astype(jnp.bfloat16)

time: 74.7 us -> 86.2 us (1.15)
  blocking collectives: 65.9 us -> 77.3 us
    all_gather x0 -> x1, blocking collectives: none -> 30.6 us  [shards(): lax.all_gather(local_out * jnp.exp(later_sum)[..., None], 'kv')]
    psum x1 -> x0, blocking collectives: 19.1 us -> none  [shards(): attended = lax.psum(local_out * jnp.exp(later_sum)[..., None], 'kv')]
where the time goes in v1:
time: 86.2 us; the launch traced here: 85.9 us
  blocking collectives  77.3 us (90%)
  matrix products  4.69 us (5%)
  between operations  1.47 us (2%)
  other arithmetic  1.38 us (2%)
  local copies, waits for them, and re-layouts  1.01 us (1%)
    all_gather x1, blocking collectives, shards(): lax.all_gather(local_out * jnp.exp(later_sum)[..., None], 'kv')  30.6 us
    psum x1, blocking collectives, shards(): summed, total_sq = lax.psum((partial_value, squares), 'kv')  23.4 us
    unnamed x1, blocking collectives  17.1 us
    psum x1, blocking collectives, shards(): return lax.psum(part_out.astype(jnp.bfloat16), 'tp')  6.23 us
    dot_general x1, matrix products, shards(): jnp.einsum('bhp,bphd->bhd', weights, value_heads, preferred_element_type=...  1.98 us

profile of v1, /device:TPU:0, one launch (start us, length us, event | category | flops | bytes accessed | tf_op | source)
XLA Modules:
  0.0 85.9 jit_solution(12941498199451985340)
XLA Ops:
  0.0 0.0 copy-start
  0.0 0.0 copy-start.4
  0.0 0.0 copy-start.1
  0.0 1.2 %fusion.19 = f32[8,128]{1,0:T(8,128)S(1)} fusion(bf16[256,128]{1,0:T(8,128)(2,1)} %param.11, bf16[8,256]{1,0:T(8,128)(2,1)} %param.9, f32[256]{0:T(256)} %param.10), kind=kOutput, calls=%fused_computation.28 | convolution fusion | flops 530432 | bytes 74752 | tf_op jit(solution)/shard_map/dot_general | solution.py:20
  1.2 0.8 fusion.18
  2.0 23.4 %all-reduce.1 = (f32[8,128]{1,0:T(8,128)S(1)}, f32[8]{0:T(128)S(1)}) all-reduce(f32[8,128]{1,0:T(8,128)S(1)} %fusion.19, f32[8]{0:T(128)S(1)} %fusion.18), channel_id=1, replica_groups=mesh['kv'=8,'tp'=4] {'kv'}, use_global_device_ids=true, to_apply=%region_0.0 | all-reduce | flops 1032 | bytes 8256 | tf_op jit(solution)/shard_map/psum | solution.py:22
  25.4 0.1 fusion.24
  25.5 0.0 copy-done
  25.5 0.6 fusion.21
  26.1 0.0 copy-start.2
  26.1 0.0 copy-start.3
  26.8 0.0 copy-done.1
  26.8 0.2 fusion.11
  27.0 0.0 copy-done.4
  27.0 0.7 dynamic-slice
  28.4 0.2 dynamic-update-slice
  28.6 17.1 %all-reduce = f32[64]{0:T(128)S(1)} all-reduce(f32[64]{0:T(128)S(1)} %dynamic-update-slice), channel_id=2, replica_groups=mesh['kv'=8,'tp'=4] {'kv'}, use_global_device_ids=true, to_apply=%add | all-reduce | flops 64 | bytes 512
  45.7 0.1 reshape.106
  45.8 0.1 select_reduce_fusion
  45.9 0.7 fusion.5
  46.7 2.0 %fusion.9 = f32[8,1,128]{2,1,0:T(1,128)S(1)} fusion(bf16[8,1024,128]{2,1,0:T(8,128)(2,1)} %param.14, bf16[8,1024,1]{1,0,2:T(8,128)(2,1)S(1)} %fusion.5), kind=kOutput, calls=%fused_computation.16 | convolution fusion | flops 2097152 | bytes 2117632 | tf_op jit(solution)/shard_map/bhp,bphd->bhd/dot_general | solution.py:42
  48.6 0.1 broadcast_multiply_fusion
  48.7 30.6 %all-gather.1 = f32[64,128]{1,0:T(8,128)S(1)} all-gather(f32[8,128]{1,0:T(8,128)S(1)} %broadcast_multiply_fusion), channel_id=3, replica_groups=mesh['kv'=8,'tp'=4] {'kv'}, dimensions={0}, use_global_device_ids=true | all-gather | bytes 36864 | tf_op jit(solution)/shard_map/all_gather | solution.py:51
  79.3 0.1 multiply_reduce_fusion
  79.5 0.0 copy-done.2
  79.5 0.0 copy-done.3
  79.5 0.2 convolution_convert_fusion
  79.7 6.2 %psum.23 = bf16[8,256]{1,0:T(8,128)(2,1)} all-reduce(bf16[8,256]{1,0:T(8,128)(2,1)S(1)} %convolution_convert_fusion), channel_id=1, replica_groups=mesh['kv'=8,'tp'=4] {'tp'}, use_global_device_ids=true, to_apply=%region_7.8 | all-reduce | flops 2048 | bytes 8192 | tf_op jit(solution)/shard_map/psum | solution.py:56
  (7 shorter events, 0.0 us)
Async XLA Ops:
  0.0 25.5 %copy-start = (bf16[8,1024,128]{2,1,0:T(8,128)(2,1)S(1)}, bf16[8,1024,128]{2,1,0:T(8,128)(2,1)}, u32[]{:S(2)}) copy-start(bf16[8,1024,128]{2,1,0:T(8,128)(2,1)} %param.13) | copy-start | bytes 6291460
  0.0 27.0 %copy-start.4 = (u32[32]{0:T(128)S(1)}, u32[32]{0:T(128)}, u32[]{:S(2)}) copy-start(u32[32]{0:T(128)} %constant.28) | copy-start | bytes 388
  0.0 26.8 %copy-start.1 = (s32[8]{0:T(128)S(1)}, s32[8]{0:T(128)}, u32[]{:S(2)}) copy-start(s32[8]{0:T(128)} %param.15) | copy-start | bytes 100
  26.1 53.4 %copy-start.2 = (bf16[128,256]{1,0:T(8,128)(2,1)S(1)}, bf16[128,256]{1,0:T(8,128)(2,1)}, u32[]{:S(2)}) copy-start(bf16[128,256]{1,0:T(8,128)(2,1)} %param.17) | copy-start | bytes 196612
  26.1 53.4 %copy-start.3 = (f32[128]{0:T(128)S(1)}, f32[128]{0:T(128)}, u32[]{:S(2)}) copy-start(f32[128]{0:T(128)} %param.16) | copy-start | bytes 1540
